TPU v7x, 32 devices: a whole 2x2x4 slice. The times are simulated.
32 devices in a mesh: kv: 16 (over z, y, x), tp: 2 (over core).
Axes of the slice: x: 2, y: 2, z: 4, core: 2. Of those that a mesh axis runs over, the one named last changes fastest.
Arguments:
- tokens: bfloat16 [64, 2048], P('tp', 'kv'), may hold values from -60 to 60
- gain_mix: float32 [2048], P('kv'), may hold values from 0.1 to 1.9
- w_query: bfloat16 [2048, 2048], P('kv', 'tp'), may hold values from -0.125 to 0.125
- w_key: bfloat16 [2048, 2048], P('kv', 'tp'), may hold values from -0.125 to 0.125
- w_value: bfloat16 [2048, 2048], P('kv', 'tp'), may hold values from -0.125 to 0.125
- w_igate: bfloat16 [2048, 8], P('kv', 'tp'), may hold values from -0.125 to 0.125
- w_fgate: bfloat16 [2048, 8], P('kv', 'tp'), may hold values from -0.125 to 0.125
- bias_igate: float32 [8], P('tp'), may hold values from -3 to 3
- bias_fgate: float32 [8], P('tp'), may hold values from -3 to 3
- state_mem: float32 [64, 8, 256, 256], P('kv', 'tp'), may hold values from -2 to 2
- state_max: float32 [64, 8], P('kv', 'tp'), may hold values from -60 to 220
- keys_blk: bfloat16 [64, 8, 128, 256], P('kv', 'tp'), may hold values from -6 to 6
- values_blk: bfloat16 [64, 8, 128, 256], P('kv', 'tp'), may hold values from -6 to 6
- igate_blk: float32 [64, 8, 128], P('kv', 'tp'), may hold values from -10 to 220
- fgate_blk: float32 [64, 8, 128], P('kv', 'tp'), may hold values from -3 to 0
- lengths: int32 [64], P('kv'), may hold values from 1 to 127, 2048 in all
- gain_head: float32 [256], replicated, may hold values from 0.1 to 1.9
- w_mixout: bfloat16 [2048, 2048], P('tp', 'kv'), may hold values from -0.25 to 0.25
- gain_mlp: float32 [2048], P('kv'), may hold values from 0.1 to 1.9
- w_up: bfloat16 [2048, 8192], P('kv', 'tp'), may hold values from -0.125 to 0.125
- w_down: bfloat16 [8192, 2048], P('tp', 'kv'), may hold values from -0.0625 to 0.0625
Outputs:
- layer_out: bfloat16 [64, 2048], P('tp', 'kv')
Inputs may be any that keep to these rules, and one draw needn't show every extreme that they name: `lengths`: entries of a sequence's block at or past its length are not live. The largest length is reached in every draw.
All inputs are finite; a program needn't handle non-finite values.
Results may differ from a plain program's by a relative error of at most 0.015.
Values may be sent and summed in bfloat16 or wider, within the bound.
No kernel may reach another device: no remote copies, remote signals or barrier semaphores. Data moves between devices by JAX's collectives and lax.ppermute only.
A program may use at most 64 MiB of HBM per device.

v0:
```python
import jax
import jax.numpy as jnp
from jax import lax
from jax.sharding import PartitionSpec as P

D = 2048


EPS = 1e-06


def memory_cell(
    query,
    key_new,
    value_new,
    input_gate,
    forget_gate,
    state_mem,
    state_max,
    keys_blk,
    values_blk,
    igate_blk,
    fgate_blk,
    lengths,
    gain_head,
):
    span = keys_blk.shape[2]
    head_size = query.shape[-1]
    positions = jnp.arange(span, dtype=jnp.int32)
    live_mask = positions[None, None, :] < lengths[:, None, None]
    forget_live = jnp.where(live_mask, fgate_blk, 0.0)
    cumulative = jnp.cumsum(forget_live, axis=-1)
    total = cumulative[..., -1]
    suffix = total[..., None] - cumulative + forget_gate[..., None]
    past = igate_blk + suffix
    carried = state_max + total + forget_gate
    topmost = jnp.maximum(
        jnp.maximum(carried, input_gate), jnp.max(jnp.where(live_mask, past, -jnp.inf), axis=-1)
    )
    scale = head_size ** (-0.5)
    scores = (
        jnp.einsum("shd,shbd->shb", query, keys_blk, preferred_element_type=jnp.float32) * scale
    )
    weights = (jnp.where(live_mask, jnp.exp(past - topmost[..., None]), 0.0) * scores).astype(
        jnp.bfloat16
    )
    block_term = jnp.einsum(
        "shb,shbd->shd", weights, values_blk, preferred_element_type=jnp.float32
    )
    query_f = query.astype(jnp.float32)
    state_term = (
        jnp.einsum("shvk,shk->shv", state_mem, query_f, precision=lax.Precision.HIGHEST)
        * jnp.exp(carried - topmost)[..., None]
    )
    own_score = jnp.sum(query_f * key_new.astype(jnp.float32), axis=-1) * scale
    own_term = (jnp.exp(input_gate - topmost) * own_score)[..., None] * value_new.astype(
        jnp.float32
    )
    numerator = state_term + block_term + own_term
    normed = (
        numerator
        * lax.rsqrt(jnp.mean(numerator * numerator, axis=-1, keepdims=True) + EPS)
        * gain_head
    )
    return normed.astype(jnp.bfloat16).reshape(query.shape[0], -1)


def body(
    tokens,
    gain_mix,
    w_query,
    w_key,
    w_value,
    w_igate,
    w_fgate,
    bias_igate,
    bias_fgate,
    state_mem,
    state_max,
    keys_blk,
    values_blk,
    igate_blk,
    fgate_blk,
    lengths,
    gain_head,
    w_mixout,
    gain_mlp,
    w_up,
    w_down,
):
    sequences = state_mem.shape[0]
    head_count = state_mem.shape[1]
    head_size = state_mem.shape[3]
    inner_width = head_count * head_size
    gathered = lax.all_gather(tokens, "tp", axis=0, tiled=True)
    widened = gathered.astype(jnp.float32)
    square_in = jnp.sum(widened * widened, axis=1)
    scaled_in = (widened * gain_mix).astype(jnp.bfloat16)
    w_main = jnp.concatenate([w_query, w_key, w_value], axis=1)
    w_gates = jnp.concatenate([w_igate, w_fgate], axis=1)
    main_part = jnp.dot(scaled_in, w_main, preferred_element_type=jnp.float32)
    gate_part = jnp.dot(scaled_in, w_gates, preferred_element_type=jnp.float32)
    square_all = lax.psum(square_in, "kv")
    square_mine = lax.dynamic_slice_in_dim(
        square_all, lax.axis_index("kv") * sequences, sequences, 0
    )
    main_sum, gate_sum = (
        lax.psum_scatter(main_part, "kv", scatter_dimension=0, tiled=True),
        lax.psum_scatter(gate_part, "kv", scatter_dimension=0, tiled=True),
    )
    factor_in = lax.rsqrt(square_mine / D + EPS)[:, None]
    projected = main_sum * factor_in
    query = (
        projected[:, :inner_width].astype(jnp.bfloat16).reshape(sequences, head_count, head_size)
    )
    key_new = (
        projected[:, inner_width : 2 * inner_width]
        .astype(jnp.bfloat16)
        .reshape(sequences, head_count, head_size)
    )
    value_new = (
        projected[:, 2 * inner_width :]
        .astype(jnp.bfloat16)
        .reshape(sequences, head_count, head_size)
    )
    gate_scaled = gate_sum * factor_in
    input_gate = gate_scaled[:, :head_count] + bias_igate
    forget_gate = jax.nn.log_sigmoid(gate_scaled[:, head_count:] + bias_fgate)
    mixed = memory_cell(
        query,
        key_new,
        value_new,
        input_gate,
        forget_gate,
        state_mem,
        state_max,
        keys_blk,
        values_blk,
        igate_blk,
        fgate_blk,
        lengths,
        gain_head,
    )
    partial_value = jnp.dot(
        lax.all_gather(mixed, "kv", axis=0, tiled=True),
        w_mixout,
        preferred_element_type=jnp.float32,
    )
    attended = lax.psum(partial_value.astype(jnp.bfloat16), "tp").astype(jnp.float32)
    residual = (widened + attended).astype(jnp.bfloat16)
    restored = residual.astype(jnp.float32)
    square_mid = jnp.sum(restored * restored, axis=1)
    scaled_mid = (restored * gain_mlp).astype(jnp.bfloat16)
    up_part = jnp.dot(scaled_mid, w_up, preferred_element_type=jnp.float32)
    up_sum, square_sum = lax.psum((up_part, square_mid), "kv")
    hidden = jnp.square(jax.nn.relu(up_sum * lax.rsqrt(square_sum / D + EPS)[:, None])).astype(
        jnp.bfloat16
    )
    down_part = jnp.dot(hidden, w_down, preferred_element_type=jnp.float32)
    down_sum = lax.psum_scatter(
        down_part.astype(jnp.bfloat16), "tp", scatter_dimension=0, tiled=True
    ).astype(jnp.float32)
    row_count = tokens.shape[0]
    own_rows = lax.dynamic_slice_in_dim(restored, lax.axis_index("tp") * row_count, row_count, 0)
    return (own_rows + down_sum).astype(jnp.bfloat16)


def solution(mesh):
    in_specs = (
        P("tp", "kv"),
        P("kv"),
        P("kv", "tp"),
        P("kv", "tp"),
        P("kv", "tp"),
        P("kv", "tp"),
        P("kv", "tp"),
        P("tp"),
        P("tp"),
        P("kv", "tp", None, None),
        P("kv", "tp"),
        P("kv", "tp", None, None),
        P("kv", "tp", None, None),
        P("kv", "tp", None),
        P("kv", "tp", None),
        P("kv"),
        P(),
        P("tp", "kv"),
        P("kv"),
        P("kv", "tp"),
        P("tp", "kv"),
    )
    out_specs = P("tp", "kv")
    return jax.shard_map(body, mesh=mesh, in_specs=in_specs, out_specs=out_specs, check_vma=False)
```

profile of v0, /device:TPU:0, one launch (start us, length us, event | category | flops | bytes accessed | tf_op | source)
XLA Modules:
  0.0 302.7 jit_solution(5341984670148661137)
XLA Ops:
  6.5 0.0 copy-start
  6.5 0.0 copy-start.12
  6.6 0.0 copy-start.11
  6.6 0.0 copy-start.8
  6.6 0.0 copy-start.5
  6.6 0.0 copy-start.9
  6.6 0.0 copy-start.7
  6.6 0.0 all-reduce.8.cloned.1.call-start
  6.7 2.3 all_gather.6
  9.0 2.4 fusion
  11.3 0.0 all-reduce.8.cloned.1.call-update
  11.4 0.0 all-reduce.6.cloned.1.call-start
  11.4 0.1 fusion.10
  11.5 0.0 copy-done.15
  11.6 0.1 iota_compare_fusion
  11.6 0.0 copy-done.6
  11.6 1.2 reduce_window_sum.11
  12.9 0.2 slice_reduce_fusion
  13.0 0.0 copy-done.13
  13.0 0.0 copy-done.12
  13.0 0.0 copy-done.11
  13.0 0.1 fusion.16
  13.2 78.7 %all-reduce.2 = (f32[64]{0:T(128)S(1)}, f32[64,8]{1,0:T(8,128)S(1)}) all-reduce(f32[64]{0:T(128)S(1)} %fusion.10, f32[64,8]{1,0:T(8,128)S(1)} %fusion.16), channel_id=1, replica_groups=mesh['kv'=16,'tp'=2] {'kv'}, use_global_device_ids=true, to_apply=%region_2.0 | all-reduce | flops 576 | bytes 4608 | tf_op jit(solution)/shard_map/psum | solution.py:103
  91.9 0.1 add_rsqrt_fusion.2
  91.9 0.0 copy-done.16
  91.9 0.6 dynamic-slice
  93.2 0.1 dynamic-slice_multiply_fusion.1
  93.3 0.0 copy-done.8
  93.3 0.1 fusion.22
  93.3 0.0 copy-done.5
  93.3 0.2 select_reduce_fusion
  93.5 0.0 copy-done.9
  93.5 0.0 copy-done.7
  93.5 0.1 subtract_exponential_fusion
  93.6 32.6 %all-reduce.8.cloned.1.call-done = f32[64,3072]{1,0:T(8,128)} async-done(((f32[64,3072]{1,0:T(8,128)}), f32[64,3072]{1,0:T(8,128)}) %all-reduce.8.cloned.1.call-update) | async-done | bytes 786448
  126.3 1.0 fusion.8
  127.3 0.0 copy-done.2
  127.3 0.4 fusion.33
  127.7 0.1 fusion.21
  127.8 0.1 multiply_reduce_fusion.2
  127.9 0.0 copy-start.10
  127.9 4.2 %fusion.32 = f32[4,4,1,256]{3,2,1,0:T(1,128)S(1)} fusion(bf16[4,4,256,1]{2,3,1,0:T(2,128)(2,1)S(1)} %reshape.65, f32[4,4,256,256]{3,2,1,0:T(8,128)} %param.30), kind=kOutput, calls=%fused_computation.61 | convolution fusion | flops 12582912 | bytes 4218880 | tf_op jit(solution)/shard_map/shvk,shk->shv/dot_general | solution.py:52
  132.1 0.0 copy-start.14
  132.2 0.0 copy-done.3
  132.2 0.2 fusion.19
  132.4 0.2 multiply_reduce_fusion.1
  132.6 0.0 copy-done.10
  132.6 0.1 multiply_convert_fusion.4
  132.7 39.3 %all-gather = bf16[16,4,1024]{2,1,0:T(4,128)(2,1)S(1)} all-gather(bf16[1,4,1024]{2,1,0:T(4,128)(2,1)S(1)} %reshape.56), channel_id=1, replica_groups=mesh['kv'=16,'tp'=2] {'kv'}, dimensions={0}, use_global_device_ids=true | all-gather | bytes 139264 | tf_op jit(solution)/shard_map/all_gather | solution.py:145
  172.0 0.0 copy-done.4
  172.1 0.2 convolution_convert_fusion.1
  172.2 3.4 %psum.29 = bf16[64,128]{1,0:T(8,128)(2,1)S(1)} all-reduce(bf16[64,128]{1,0:T(8,128)(2,1)S(1)} %convolution_convert_fusion.1), channel_id=1, replica_groups=mesh['kv'=16,'tp'=2] {'tp'}, use_global_device_ids=true, to_apply=%region_8.9 | all-reduce | flops 8192 | bytes 32768 | tf_op jit(solution)/shard_map/psum | solution.py:149
  175.6 0.0 copy-done.14
  175.6 0.0 copy-start.1
  175.6 1.3 fusion.12
  177.0 0.0 all-reduce.6.cloned.1.call-update
  177.0 0.0 reduce-scatter.2.cloned.1.call-start
  177.0 0.1 fusion.13
  177.1 36.8 %psum.31 = f32[64]{0:T(128)S(1)} all-reduce(f32[64]{0:T(128)S(1)} %get-tuple-element.12), channel_id=1, replica_groups=mesh['kv'=16,'tp'=2] {'kv'}, use_global_device_ids=true, to_apply=%region_11.12 | all-reduce | flops 64 | bytes 512 | tf_op jit(solution)/shard_map/psum | solution.py:155
  214.0 71.9 %all-reduce.6.cloned.1.call-done = f32[64,4096]{1,0:T(8,128)} async-done(((f32[64,4096]{1,0:T(8,128)}), f32[64,4096]{1,0:T(8,128)}) %all-reduce.6.cloned.1.call-update) | async-done | bytes 1048592 | tf_op jit(solution)/shard_map/psum | solution.py:155
  285.9 2.2 convolution_convert_fusion
  288.1 0.0 reduce-scatter.2.cloned.1.call-update
  288.1 6.7 %reduce-scatter.2.cloned.1.call-done = bf16[32,128]{1,0:T(8,128)(2,1)} async-done(((bf16[64,128]{1,0:T(8,128)(2,1)}), bf16[32,128]{1,0:T(8,128)(2,1)}) %reduce-scatter.2.cloned.1.call-update) | async-done | bytes 8208 | tf_op jit(solution)/shard_map/reduce_scatter | solution.py:160
  294.8 1.3 add_convert_fusion
  (20 shorter events, 0.2 us)
Async XLA Ops:
  6.5 169.1 %copy-start = (bf16[128,4096]{1,0:T(8,128)(2,1)S(1)}, bf16[128,4096]{1,0:T(8,128)(2,1)}, u32[]{:S(2)}) copy-start(bf16[128,4096]{1,0:T(8,128)(2,1)} %param.40) | copy-start | bytes 3145732
  6.5 85.4 %copy-start.16 = (u32[32]{0:T(128)S(1)}, u32[32]{0:T(128)}, u32[]{:S(2)}) copy-start(u32[32]{0:T(128)} %constant.52) | copy-start | bytes 388
  6.5 6.5 %copy-start.13 = (f32[128]{0:T(128)S(1)}, f32[128]{0:T(128)}, u32[]{:S(2)}) copy-start(f32[128]{0:T(128)} %param.22) | copy-start | bytes 1540
  6.5 5.0 %copy-start.15 = (s32[4]{0:T(128)S(1)}, s32[4]{0:T(128)}, u32[]{:S(2)}) copy-start(s32[4]{0:T(128)} %param.36) | copy-start | bytes 52
  6.5 5.1 %copy-start.6 = (f32[4,4,128]{2,1,0:T(4,128)S(1)}, f32[4,4,128]{2,1,0:T(4,128)}, u32[]{:S(2)}) copy-start(f32[4,4,128]{2,1,0:T(4,128)} %param.35) | copy-start | bytes 24580
  6.5 6.5 %copy-start.12 = (bf16[128,4]{0,1:T(4,128)(2,1)S(1)}, bf16[128,4]{0,1:T(4,128)(2,1)}, u32[]{:S(2)}) copy-start(bf16[128,4]{0,1:T(4,128)(2,1)} %param.26) | copy-start | bytes 3076
  6.6 6.5 %copy-start.11 = (bf16[128,4]{0,1:T(4,128)(2,1)S(1)}, bf16[128,4]{0,1:T(4,128)(2,1)}, u32[]{:S(2)}) copy-start(bf16[128,4]{0,1:T(4,128)(2,1)} %param.27) | copy-start | bytes 3076
  6.6 86.7 %copy-start.8 = (f32[4]{0:T(128)S(1)}, f32[4]{0:T(128)}, u32[]{:S(2)}) copy-start(f32[4]{0:T(128)} %param.29) | copy-start | bytes 52
  6.6 86.8 %copy-start.5 = (f32[4,4,128]{2,1,0:T(4,128)S(1)}, f32[4,4,128]{2,1,0:T(4,128)}, u32[]{:S(2)}) copy-start(f32[4,4,128]{2,1,0:T(4,128)} %param.34) | copy-start | bytes 24580
  6.6 86.9 %copy-start.9 = (f32[4]{0:T(128)S(1)}, f32[4]{0:T(128)}, u32[]{:S(2)}) copy-start(f32[4]{0:T(128)} %param.28) | copy-start | bytes 52
  6.6 86.9 %copy-start.7 = (f32[4,4]{1,0:T(4,128)S(1)}, f32[4,4]{1,0:T(4,128)}, u32[]{:S(2)}) copy-start(f32[4,4]{1,0:T(4,128)} %param.31) | copy-start | bytes 196
  6.6 119.6 %all-reduce.8.cloned.1.call-start = ((), (), s32[]{:S(2)}) async-start(), calls=%async_computation.3 | async-start | bytes 1572864
  9.0 118.3 %copy-start.2 = (bf16[4,4,128,256]{3,2,1,0:T(8,128)(2,1)S(1)}, bf16[4,4,128,256]{3,2,1,0:T(8,128)(2,1)}, u32[]{:S(2)}) copy-start(bf16[4,4,128,256]{3,2,1,0:T(8,128)(2,1)} %param.32) | copy-start | bytes 3145732
  11.4 274.5 %all-reduce.6.cloned.1.call-start = ((), (), s32[]{:S(2)}) async-start(), calls=%async_computation.1 | async-start | bytes 2097152 | tf_op jit(solution)/shard_map/psum | solution.py:155
  127.9 4.3 %copy-start.3 = (bf16[4,4,128,256]{3,2,1,0:T(8,128)(2,1)S(1)}, bf16[4,4,128,256]{3,2,1,0:T(8,128)(2,1)}, u32[]{:S(2)}) copy-start(bf16[4,4,128,256]{3,2,1,0:T(8,128)(2,1)} %param.33) | copy-start | bytes 3145732
  127.9 4.7 %copy-start.10 = (f32[256]{0:T(256)S(1)}, f32[256]{0:T(256)}, u32[]{:S(2)}) copy-start(f32[256]{0:T(256)} %param.37) | copy-start | bytes 3076
  132.1 39.9 %copy-start.4 = (bf16[1024,128]{1,0:T(8,128)(2,1)S(1)}, bf16[1024,128]{1,0:T(8,128)(2,1)}, u32[]{:S(2)}) copy-start(bf16[1024,128]{1,0:T(8,128)(2,1)} %param.38) | copy-start | bytes 786436
  132.1 43.5 %copy-start.14 = (f32[128]{0:T(128)S(1)}, f32[128]{0:T(128)}, u32[]{:S(2)}) copy-start(f32[128]{0:T(128)} %param.39) | copy-start | bytes 1540
  175.6 110.3 %copy-start.1 = (bf16[4096,128]{1,0:T(8,128)(2,1)S(1)}, bf16[4096,128]{1,0:T(8,128)(2,1)}, u32[]{:S(2)}) copy-start(bf16[4096,128]{1,0:T(8,128)(2,1)} %param.41) | copy-start | bytes 3145732
  177.0 117.9 %reduce-scatter.2.cloned.1.call-start = ((), (), s32[]{:S(2)}) async-start(), calls=%async_computation.2 | async-start | bytes 24576 | tf_op jit(solution)/shard_map/reduce_scatter | solution.py:160
Sparse Core Ops, SparseCore 0:
  12.6 113.5 all-reduce.7
  177.1 108.7 all-reduce.5
  288.2 6.5 reduce-scatter.1
where the time goes:
time: 303 us
  blocking collectives  160 us (53%)
  waiting for transfers between devices  111 us (37%)
  between operations  14 us (5%)
  matrix products  11 us (4%)
  other arithmetic  4.75 us (2%)
    psum x1, blocking collectives, body(): square_all = lax.psum(square_in, 'kv')  78.7 us
    psum x1, waiting for transfers between devices, body(): up_sum, square_sum = lax.psum((up_part, square_mid), 'kv')  71.9 us
    all_gather x1, blocking collectives, body(): lax.all_gather(mixed, 'kv', axis=0, tiled=True)  39.3 us
    psum x1, blocking collectives, body(): up_sum, square_sum = lax.psum((up_part, square_mid), 'kv')  36.8 us
    unnamed x4, waiting for transfers between devices  32.7 us
    reduce_scatter x1, waiting for transfers between devices, body(): lax.psum_scatter(down_part.astype(jnp.bfloat16), 'tp', scatter_dimension=...  6.74 us
  transfers between devices with their start and end apart: 3, of which 3 were waited for; matrix products, arithmetic and copies ran while one was open for 1% of the time, Pallas kernels for 0%

commit v1 on v0

--- a/solution.py
+++ b/solution.py
@@ -7,6 +7,7 @@
 
 
 EPS = 1e-06
+LANES = 128
 
 
 def memory_cell(
@@ -63,6 +64,57 @@
         * gain_head
     )
     return normed.astype(jnp.bfloat16).reshape(query.shape[0], -1)
+
+
+def pieces(values):
+    first = lax.reduce_precision(values, 8, 7)
+    rest = values - first
+    second = lax.reduce_precision(rest, 8, 7)
+    third = lax.reduce_precision(rest - second, 8, 7)
+    return jnp.concatenate([first, second, third], axis=1).astype(jnp.bfloat16)
+
+
+def with_extras(main, extras):
+    packed = pieces(extras)
+    pad = -packed.shape[1] % LANES
+    return jnp.concatenate(
+        [main.astype(jnp.bfloat16), jnp.pad(packed, ((0, 0), (0, pad)))], axis=1
+    )
+
+
+def scatter_sum(packed, width, extra_count):
+    peers = lax.axis_size("kv")
+    blocks = packed.reshape(peers, packed.shape[0] // peers, packed.shape[1])
+    received = lax.all_to_all(blocks, "kv", 0, 0, tiled=True)
+    total = jnp.sum(received.astype(jnp.float32), axis=0)
+    extras = total[:, width : width + 3 * extra_count]
+    extras = extras.reshape(total.shape[0], 3, extra_count)
+    return total[:, :width], extras[:, 0] + (extras[:, 1] + extras[:, 2])
+
+
+def gather_rows(rows):
+    peers = lax.axis_size("kv")
+    copies = jnp.broadcast_to(rows[None], (peers,) + rows.shape)
+    return lax.all_to_all(copies, "kv", 0, 0, tiled=True).reshape(-1, rows.shape[1])
+
+
+def tp_sum(partial):
+    if lax.axis_size("tp") != 2:
+        return lax.psum(partial, "tp").astype(jnp.float32)
+    other = lax.ppermute(partial, "tp", [(0, 1), (1, 0)])
+    return partial.astype(jnp.float32) + other.astype(jnp.float32)
+
+
+def tp_scatter_sum(partial, row_count):
+    if lax.axis_size("tp") != 2:
+        return lax.psum_scatter(partial, "tp", scatter_dimension=0, tiled=True).astype(
+            jnp.float32
+        )
+    side = lax.axis_index("tp")
+    own = lax.dynamic_slice_in_dim(partial, side * row_count, row_count, 0)
+    away = lax.dynamic_slice_in_dim(partial, (1 - side) * row_count, row_count, 0)
+    other = lax.ppermute(away, "tp", [(0, 1), (1, 0)])
+    return own.astype(jnp.float32) + other.astype(jnp.float32)
 
 
 def body(
@@ -100,14 +152,12 @@
     w_gates = jnp.concatenate([w_igate, w_fgate], axis=1)
     main_part = jnp.dot(scaled_in, w_main, preferred_element_type=jnp.float32)
     gate_part = jnp.dot(scaled_in, w_gates, preferred_element_type=jnp.float32)
-    square_all = lax.psum(square_in, "kv")
-    square_mine = lax.dynamic_slice_in_dim(
-        square_all, lax.axis_index("kv") * sequences, sequences, 0
-    )
-    main_sum, gate_sum = (
-        lax.psum_scatter(main_part, "kv", scatter_dimension=0, tiled=True),
-        lax.psum_scatter(gate_part, "kv", scatter_dimension=0, tiled=True),
-    )
+    extras_in = jnp.concatenate([gate_part, square_in[:, None]], axis=1)
+    main_sum, extra_sum = scatter_sum(
+        with_extras(main_part, extras_in), main_part.shape[1], extras_in.shape[1]
+    )
+    gate_sum = extra_sum[:, : 2 * head_count]
+    square_mine = extra_sum[:, 2 * head_count]
     factor_in = lax.rsqrt(square_mine / D + EPS)[:, None]
     projected = main_sum * factor_in
     query = (
@@ -142,25 +192,23 @@
         gain_head,
     )
     partial_value = jnp.dot(
-        lax.all_gather(mixed, "kv", axis=0, tiled=True),
+        gather_rows(mixed),
         w_mixout,
         preferred_element_type=jnp.float32,
     )
-    attended = lax.psum(partial_value.astype(jnp.bfloat16), "tp").astype(jnp.float32)
+    attended = tp_sum(partial_value.astype(jnp.bfloat16))
     residual = (widened + attended).astype(jnp.bfloat16)
     restored = residual.astype(jnp.float32)
-    square_mid = jnp.sum(restored * restored, axis=1)
+    square_mid = jnp.sum(restored * restored, axis=1, keepdims=True)
     scaled_mid = (restored * gain_mlp).astype(jnp.bfloat16)
     up_part = jnp.dot(scaled_mid, w_up, preferred_element_type=jnp.float32)
-    up_sum, square_sum = lax.psum((up_part, square_mid), "kv")
-    hidden = jnp.square(jax.nn.relu(up_sum * lax.rsqrt(square_sum / D + EPS)[:, None])).astype(
+    up_sum, square_sum = scatter_sum(with_extras(up_part, square_mid), up_part.shape[1], 1)
+    hidden = jnp.square(jax.nn.relu(up_sum * lax.rsqrt(square_sum / D + EPS))).astype(
         jnp.bfloat16
     )
-    down_part = jnp.dot(hidden, w_down, preferred_element_type=jnp.float32)
-    down_sum = lax.psum_scatter(
-        down_part.astype(jnp.bfloat16), "tp", scatter_dimension=0, tiled=True
-    ).astype(jnp.float32)
+    down_part = jnp.dot(gather_rows(hidden), w_down, preferred_element_type=jnp.float32)
     row_count = tokens.shape[0]
+    down_sum = tp_scatter_sum(down_part.astype(jnp.bfloat16), row_count)
     own_rows = lax.dynamic_slice_in_dim(restored, lax.axis_index("tp") * row_count, row_count, 0)
     return (own_rows + down_sum).astype(jnp.bfloat16)
 

time: 303 us -> 89.2 us (0.29)
  blocking collectives: 160 us -> 33.3 us
  waiting for transfers between devices: 111 us -> 28.5 us
  between operations: 14 us -> 0.36 us
  starting transfers between devices: 0.12 us -> 11.9 us
  matrix products: 11 us -> 7.85 us
    psum x3 -> x0, blocking collectives: 119 us -> none  [the longest x1 78.7 us: body(): square_all = lax.psum(square_in, 'kv')]
    psum x1 -> x0, waiting for transfers between devices: 71.9 us -> none  [body(): up_sum, square_sum = lax.psum((up_part, square_mid), 'kv')]
    all_gather x1 -> x0, blocking collectives: 39.3 us -> none  [body(): lax.all_gather(mixed, 'kv', axis=0, tiled=True)]
    unnamed x4 -> x0, waiting for transfers between devices: 32.7 us -> none
    all_to_all x0 -> x2, blocking collectives: none -> 31 us  [the longest x1 19.7 us: scatter_sum(): received = lax.all_to_all(blocks, 'kv', 0, 0, tiled=True)]
    all_to_all x0 -> x2, waiting for transfers between devices: none -> 26.2 us  [the longest x1 14.5 us: gather_rows(): lax.all_to_all(copies, 'kv', 0, 0, tiled=True).reshape(-1, rows.shape[1])]
    all_to_all x0 -> x2, starting transfers between devices: none -> 11.8 us  [the longest x1 8.19 us: scatter_sum(): received = lax.all_to_all(blocks, 'kv', 0, 0, tiled=True)]
    reduce_scatter x1 -> x0, waiting for transfers between devices: 6.74 us -> none  [body(): lax.psum_scatter(down_part.astype(jnp.bfloat16), 'tp', scatter_dimension=...]
  transfers between devices with their start and end apart: 3 -> 4, of which waited for: 3 -> 4; matrix products, arithmetic and copies ran while one was open for 1% -> 2% of each run, Pallas kernels for 0% -> 0%
where the time goes in v1:
time: 89.2 us; the launch traced here: 88.8 us
  blocking collectives  33.3 us (37%)
  waiting for transfers between devices  28.5 us (32%)
  starting transfers between devices  11.9 us (13%)
  matrix products  7.85 us (9%)
  other arithmetic  4.1 us (5%)
  local copies, waits for them, and re-layouts  2.79 us (3%)
    all_to_all x1, blocking collectives, scatter_sum(): received = lax.all_to_all(blocks, 'kv', 0, 0, tiled=True)  19.7 us
    all_to_all x1, waiting for transfers between devices, gather_rows(): lax.all_to_all(copies, 'kv', 0, 0, tiled=True).reshape(-1, rows.shape[1])  14.5 us
    all_to_all x1, waiting for transfers between devices, scatter_sum(): received = lax.all_to_all(blocks, 'kv', 0, 0, tiled=True)  11.8 us
    all_to_all x1, blocking collectives, gather_rows(): lax.all_to_all(copies, 'kv', 0, 0, tiled=True).reshape(-1, rows.shape[1])  11.3 us
    all_to_all x1, starting transfers between devices, scatter_sum(): received = lax.all_to_all(blocks, 'kv', 0, 0, tiled=True)  8.19 us
    dot_general x1, matrix products, memory_cell(): jnp.einsum('shvk,shk->shv', state_mem, query_f, precision=lax.Precision.H...  4.22 us
    all_to_all x1, starting transfers between devices, gather_rows(): lax.all_to_all(copies, 'kv', 0, 0, tiled=True).reshape(-1, rows.shape[1])  3.57 us
    all_gather x1, blocking collectives, body(): gathered = lax.all_gather(tokens, 'tp', axis=0, tiled=True)  2.3 us
  transfers between devices with their start and end apart: 4, of which 4 were waited for; matrix products, arithmetic and copies ran while one was open for 2% of the time, Pallas kernels for 0%

profile of v1, /device:TPU:0, one launch (start us, length us, event | category | flops | bytes accessed | tf_op | source)
XLA Modules:
  0.0 88.8 jit_solution(8268069337017978871)
XLA Ops:
  0.0 0.0 copy-start
  0.0 2.3 %all_gather.3 = bf16[64,128]{1,0:T(8,128)(2,1)S(1)} all-gather(bf16[32,128]{1,0:T(8,128)(2,1)} %param.21), channel_id=1, replica_groups=mesh['kv'=16,'tp'=2] {'tp'}, dimensions={0}, use_global_device_ids=true | all-gather | bytes 24576 | tf_op jit(solution)/shard_map/all_gather | solution.py:147
  2.3 0.1 fusion.14
  2.4 0.8 fusion.19
  3.3 0.1 copy.40
  3.4 1.4 %convolution_convert_fusion.1 = bf16[64,3072]{1,0:T(8,128)(2,1)S(1)} fusion(bf16[128,1024]{1,0:T(8,128)(2,1)} %param.25, bf16[128,1024]{1,0:T(8,128)(2,1)} %param.24, bf16[128,1024]{1,0:T(8,128)(2,1)} %param.23, bf16[64,128]{1,0:T(8,128)(2,1)S(1)} %all_gather.3, f32[128]{0:T(128)} %param.22), kind=kOutput, calls=%fused_computation.1 | convolution fusion | flops 52912128 | bytes 1196544 | tf_op jit(solution)/shard_map/dot_general | solution.py:153
  4.8 0.0 copy-start.12
  4.8 0.0 copy-start.6
  4.8 0.0 copy-start.8
  4.8 0.0 copy-start.2
  4.9 0.0 copy-start.5
  4.9 0.0 copy-start.7
  4.9 0.0 copy-start.9
  4.9 0.8 reshape.132
  5.8 8.2 %all-to-all-start = ((bf16[16,4,3200]{2,1,0:T(4,128)(2,1)}), bf16[16,4,3200]{2,1,0:T(4,128)(2,1)S(1)}, u32[]{:S(2)}, u32[]{:S(2)}) async-start(bf16[16,4,3200]{2,1,0:T(4,128)(2,1)} %reshape.132), calls=%async_computation | async-start | bytes 819200 | tf_op jit(solution)/shard_map/all_to_all | solution.py:88
  14.0 0.0 copy-done.12
  14.0 0.1 iota_compare_fusion.2
  14.0 0.0 copy-done.6
  14.1 1.2 %reduce_window_sum.11 = f32[4,4,128]{2,1,0:T(4,128)S(1)} reduce-window(f32[4,4,128]{2,1,0:T(4,128)S(1)} %broadcast_select_fusion, f32[]{:T(128)} %constant.12.clone.1), window={size=1x1x128 pad=0_0x0_0x127_0}, to_apply=%region_2.3 | reduce-window | flops 260096 | bytes 16388 | tf_op jit(solution)/shard_map/jit(cumsum)/reduce_window_sum | solution.py:33
  15.3 0.2 slice_reduce_fusion
  15.4 11.8 %all-to-all-done = bf16[16,4,3200]{2,1,0:T(4,128)(2,1)S(1)} async-done(((bf16[16,4,3200]{2,1,0:T(4,128)(2,1)}), bf16[16,4,3200]{2,1,0:T(4,128)(2,1)S(1)}, u32[]{:S(2)}, u32[]{:S(2)}) %all-to-all-start) | async-done | bytes 409632 | tf_op jit(solution)/shard_map/all_to_all | solution.py:88
  27.2 0.2 convert_reduce_fusion.1
  27.4 0.1 reshape.133
  27.5 0.2 rsqrt_reduce_fusion.1
  27.7 0.1 slice_multiply_fusion.2
  27.7 0.1 fusion.12
  27.9 0.1 fusion.28
  28.0 0.0 copy-done.2
  28.0 0.4 fusion.41
  28.4 0.0 copy-done.5
  28.4 0.2 select_reduce_fusion
  28.6 0.0 copy-done.9
  28.6 0.1 subtract_exponential_fusion
  28.7 0.1 fusion.27
  28.8 0.1 multiply_reduce_fusion.2
  28.9 0.0 copy-start.10
  28.9 4.2 %fusion.40 = f32[4,4,1,256]{3,2,1,0:T(1,128)S(1)} fusion(bf16[4,4,256,1]{2,3,1,0:T(2,128)(2,1)S(1)} %reshape.148, f32[4,4,256,256]{3,2,1,0:T(8,128)} %param.30), kind=kOutput, calls=%fused_computation.89 | convolution fusion | flops 12582912 | bytes 4218880 | tf_op jit(solution)/shard_map/shvk,shk->shv/dot_general | solution.py:53
  33.1 0.0 copy-start.11
  33.2 0.2 fusion.25
  33.4 0.2 multiply_reduce_fusion.1
  33.6 0.0 copy-done.10
  33.6 0.1 fusion.24
  33.7 11.3 %all_to_all.20 = bf16[16,4,1024]{2,1,0:T(4,128)(2,1)S(1)} all-to-all(bf16[16,4,1024]{2,1,0:T(4,128)(2,1)S(1)} %broadcast_in_dim.57), channel_id=1, replica_groups=mesh['kv'=16,'tp'=2] {'kv'}, dimensions={0} | all-to-all | bytes 262144 | tf_op jit(solution)/shard_map/all_to_all | solution.py:98
  45.0 0.0 copy-done.4
  45.0 0.2 convolution_convert_fusion.3
  45.2 0.1 collective-permute-start
  45.3 1.2 %collective-permute-done = bf16[64,128]{1,0:T(8,128)(2,1)S(1)} collective-permute-done((bf16[64,128]{1,0:T(8,128)(2,1)S(1)}, bf16[64,128]{1,0:T(8,128)(2,1)S(1)}, u32[]{:S(2)}, u32[]{:S(2)}) %collective-permute-start) | collective-permute-done | bytes 16416 | tf_op jit(solution)/shard_map/ppermute | solution.py:104
  46.5 0.1 multiply_reduce_fusion
  46.6 0.1 copy.34
  46.7 0.3 convolution_convert_fusion
  47.1 0.1 reshape.136
  47.2 19.7 %all_to_all.21 = bf16[16,4,4224]{2,1,0:T(4,128)(2,1)S(1)} all-to-all(bf16[16,4,4224]{2,1,0:T(4,128)(2,1)S(1)} %reshape.136), channel_id=1, replica_groups=mesh['kv'=16,'tp'=2] {'kv'}, dimensions={0} | all-to-all | bytes 1081344 | tf_op jit(solution)/shard_map/all_to_all | solution.py:88
  66.9 0.2 convert_reduce_fusion
  67.2 0.2 rsqrt_reduce_fusion
  67.4 0.1 fusion.11
  67.5 1.0 %broadcast_in_dim.58 = bf16[16,4,4096]{2,1,0:T(4,128)(2,1)} broadcast(bf16[4,4096]{1,0:T(4,128)(2,1)S(1)} %fusion.11), dimensions={1,2} | broadcast | bytes 557056 | tf_op jit(solution)/shard_map/broadcast_in_dim | solution.py:97
  68.5 3.6 %all-to-all-start.3 = ((bf16[16,4,4096]{2,1,0:T(4,128)(2,1)}), bf16[16,4,4096]{2,1,0:T(4,128)(2,1)S(1)}, u32[]{:S(2)}, u32[]{:S(2)}) async-start(bf16[16,4,4096]{2,1,0:T(4,128)(2,1)} %broadcast_in_dim.58), calls=%async_computation.3 | async-start | bytes 1048576 | tf_op jit(solution)/shard_map/all_to_all | solution.py:98
  72.0 14.5 %all-to-all-done.3 = bf16[16,4,4096]{2,1,0:T(4,128)(2,1)S(1)} async-done(((bf16[16,4,4096]{2,1,0:T(4,128)(2,1)}), bf16[16,4,4096]{2,1,0:T(4,128)(2,1)S(1)}, u32[]{:S(2)}, u32[]{:S(2)}) %all-to-all-start.3) | async-done | bytes 524320 | tf_op jit(solution)/shard_map/all_to_all | solution.py:98
  86.5 0.1 reshape.138
  86.6 0.0 copy-done.1
  86.6 0.3 convolution_convert_fusion.2
  87.0 0.1 collective-permute-start.1
  87.0 1.2 %collective-permute-done.1 = bf16[32,128]{1,0:T(8,128)(2,1)S(1)} collective-permute-done((bf16[32,128]{1,0:T(8,128)(2,1)S(1)}, bf16[32,128]{1,0:T(8,128)(2,1)S(1)}, u32[]{:S(2)}, u32[]{:S(2)}) %collective-permute-start.1) | collective-permute-done | bytes 8224 | tf_op jit(solution)/shard_map/ppermute | solution.py:116
  88.2 0.6 add_convert_fusion
  (29 shorter events, 0.3 us)
Async XLA Ops:
  0.0 46.7 %copy-start = (bf16[128,4096]{1,0:T(8,128)(2,1)S(1)}, bf16[128,4096]{1,0:T(8,128)(2,1)}, u32[]{:S(2)}) copy-start(bf16[128,4096]{1,0:T(8,128)(2,1)} %param.40) | copy-start | bytes 3145732
  4.8 9.2 %copy-start.12 = (s32[4]{0:T(128)S(1)}, s32[4]{0:T(128)}, u32[]{:S(2)}) copy-start(s32[4]{0:T(128)} %param.36) | copy-start | bytes 52
  4.8 9.2 %copy-start.6 = (f32[4,4,128]{2,1,0:T(4,128)S(1)}, f32[4,4,128]{2,1,0:T(4,128)}, u32[]{:S(2)}) copy-start(f32[4,4,128]{2,1,0:T(4,128)} %param.35) | copy-start | bytes 24580
  4.8 23.1 %copy-start.8 = (f32[4]{0:T(128)S(1)}, f32[4]{0:T(128)}, u32[]{:S(2)}) copy-start(f32[4]{0:T(128)} %param.29) | copy-start | bytes 52
  4.8 23.2 %copy-start.2 = (bf16[4,4,128,256]{3,2,1,0:T(8,128)(2,1)S(1)}, bf16[4,4,128,256]{3,2,1,0:T(8,128)(2,1)}, u32[]{:S(2)}) copy-start(bf16[4,4,128,256]{3,2,1,0:T(8,128)(2,1)} %param.32) | copy-start | bytes 3145732
  4.9 23.5 %copy-start.5 = (f32[4,4,128]{2,1,0:T(4,128)S(1)}, f32[4,4,128]{2,1,0:T(4,128)}, u32[]{:S(2)}) copy-start(f32[4,4,128]{2,1,0:T(4,128)} %param.34) | copy-start | bytes 24580
  4.9 23.7 %copy-start.7 = (f32[4,4]{1,0:T(4,128)S(1)}, f32[4,4]{1,0:T(4,128)}, u32[]{:S(2)}) copy-start(f32[4,4]{1,0:T(4,128)} %param.31) | copy-start | bytes 196
  4.9 23.6 %copy-start.9 = (f32[4]{0:T(128)S(1)}, f32[4]{0:T(128)}, u32[]{:S(2)}) copy-start(f32[4]{0:T(128)} %param.28) | copy-start | bytes 52
  5.8 21.4 %all-to-all-start = ((bf16[16,4,3200]{2,1,0:T(4,128)(2,1)}), bf16[16,4,3200]{2,1,0:T(4,128)(2,1)S(1)}, u32[]{:S(2)}, u32[]{:S(2)}) async-start(bf16[16,4,3200]{2,1,0:T(4,128)(2,1)} %reshape.132), calls=%async_computation | async-start | bytes 819200 | tf_op jit(solution)/shard_map/all_to_all | solution.py:88
  28.9 4.3 %copy-start.3 = (bf16[4,4,128,256]{3,2,1,0:T(8,128)(2,1)S(1)}, bf16[4,4,128,256]{3,2,1,0:T(8,128)(2,1)}, u32[]{:S(2)}) copy-start(bf16[4,4,128,256]{3,2,1,0:T(8,128)(2,1)} %param.33) | copy-start | bytes 3145732
  28.9 4.7 %copy-start.10 = (f32[256]{0:T(256)S(1)}, f32[256]{0:T(256)}, u32[]{:S(2)}) copy-start(f32[256]{0:T(256)} %param.37) | copy-start | bytes 3076
  33.1 11.9 %copy-start.4 = (bf16[1024,128]{1,0:T(8,128)(2,1)S(1)}, bf16[1024,128]{1,0:T(8,128)(2,1)}, u32[]{:S(2)}) copy-start(bf16[1024,128]{1,0:T(8,128)(2,1)} %param.38) | copy-start | bytes 786436
  33.1 13.6 %copy-start.11 = (f32[128]{0:T(128)S(1)}, f32[128]{0:T(128)}, u32[]{:S(2)}) copy-start(f32[128]{0:T(128)} %param.39) | copy-start | bytes 1540
  45.2 1.2 %collective-permute-start = (bf16[64,128]{1,0:T(8,128)(2,1)S(1)}, bf16[64,128]{1,0:T(8,128)(2,1)S(1)}, u32[]{:S(2)}, u32[]{:S(2)}) collective-permute-start(bf16[64,128]{1,0:T(8,128)(2,1)S(1)} %convolution_convert_fusion.3), channel_id=1, source_target_pairs={{0,1},{1,0},{2,3},{3,2},{4,5},{5,4},{6,7},{7,6},{8,9},{9,8},{10,11... | collective-permute-start | bytes 49160 | tf_op jit(solution)/shard_map/ppermute | solution.py:104
  66.9 19.7 %copy-start.1 = (bf16[4096,128]{1,0:T(8,128)(2,1)S(1)}, bf16[4096,128]{1,0:T(8,128)(2,1)}, u32[]{:S(2)}) copy-start(bf16[4096,128]{1,0:T(8,128)(2,1)} %param.41) | copy-start | bytes 3145732
  68.5 18.0 %all-to-all-start.3 = ((bf16[16,4,4096]{2,1,0:T(4,128)(2,1)}), bf16[16,4,4096]{2,1,0:T(4,128)(2,1)S(1)}, u32[]{:S(2)}, u32[]{:S(2)}) async-start(bf16[16,4,4096]{2,1,0:T(4,128)(2,1)} %broadcast_in_dim.58), calls=%async_computation.3 | async-start | bytes 1048576 | tf_op jit(solution)/shard_map/all_to_all | solution.py:98
  87.0 1.2 %collective-permute-start.1 = (bf16[32,128]{1,0:T(8,128)(2,1)S(1)}, bf16[32,128]{1,0:T(8,128)(2,1)S(1)}, u32[]{:S(2)}, u32[]{:S(2)}) collective-permute-start(bf16[32,128]{1,0:T(8,128)(2,1)S(1)} %constant_dynamic-slice_fusion), channel_id=1, source_target_pairs={{0,1},{1,0},{2,3},{3,2},{4,5},{5,4},{6,7},{7,6},{8,9},{9,8},{10,11... | collective-permute-start | bytes 24584 | tf_op jit(solution)/shard_map/ppermute | solution.py:116

commit v2 on v1

--- a/solution.py
+++ b/solution.py
@@ -21,18 +21,13 @@
     keys_blk,
     values_blk,
     igate_blk,
-    fgate_blk,
-    lengths,
+    live_mask,
+    later,
+    total,
     gain_head,
 ):
-    span = keys_blk.shape[2]
     head_size = query.shape[-1]
-    positions = jnp.arange(span, dtype=jnp.int32)
-    live_mask = positions[None, None, :] < lengths[:, None, None]
-    forget_live = jnp.where(live_mask, fgate_blk, 0.0)
-    cumulative = jnp.cumsum(forget_live, axis=-1)
-    total = cumulative[..., -1]
-    suffix = total[..., None] - cumulative + forget_gate[..., None]
+    suffix = later + forget_gate[..., None]
     past = igate_blk + suffix
     carried = state_max + total + forget_gate
     topmost = jnp.maximum(
@@ -50,7 +45,12 @@
     )
     query_f = query.astype(jnp.float32)
     state_term = (
-        jnp.einsum("shvk,shk->shv", state_mem, query_f, precision=lax.Precision.HIGHEST)
+        jnp.einsum(
+            "shvk,shk->shv",
+            state_mem.astype(jnp.bfloat16),
+            query,
+            preferred_element_type=jnp.float32,
+        )
         * jnp.exp(carried - topmost)[..., None]
     )
     own_score = jnp.sum(query_f * key_new.astype(jnp.float32), axis=-1) * scale
@@ -105,16 +105,35 @@
     return partial.astype(jnp.float32) + other.astype(jnp.float32)
 
 
-def tp_scatter_sum(partial, row_count):
+def half_of(rows, row_count, lower):
+    return jnp.where(lower, rows[:row_count], rows[row_count:])
+
+
+def own_half(rows, row_count, first_side):
+    if lax.axis_size("tp") != 2:
+        return lax.dynamic_slice_in_dim(rows, lax.axis_index("tp") * row_count, row_count, 0)
+    return half_of(rows, row_count, first_side)
+
+
+def tp_scatter_sum(partial, row_count, first_side):
     if lax.axis_size("tp") != 2:
         return lax.psum_scatter(partial, "tp", scatter_dimension=0, tiled=True).astype(
             jnp.float32
         )
-    side = lax.axis_index("tp")
-    own = lax.dynamic_slice_in_dim(partial, side * row_count, row_count, 0)
-    away = lax.dynamic_slice_in_dim(partial, (1 - side) * row_count, row_count, 0)
+    own = half_of(partial, row_count, first_side)
+    away = jnp.where(first_side, partial[row_count:], partial[:row_count])
     other = lax.ppermute(away, "tp", [(0, 1), (1, 0)])
     return own.astype(jnp.float32) + other.astype(jnp.float32)
+
+
+def block_gates(fgate_blk, lengths):
+    span = fgate_blk.shape[2]
+    positions = jnp.arange(span, dtype=jnp.int32)
+    live_mask = positions[None, None, :] < lengths[:, None, None]
+    forget_live = jnp.where(live_mask, fgate_blk, 0.0)
+    after = (positions[:, None] > positions[None, :]).astype(jnp.float32)
+    later = jnp.einsum("shj,jp->shp", forget_live, after, precision=lax.Precision.HIGHEST)
+    return live_mask, later, jnp.sum(forget_live, axis=-1)
 
 
 def body(
@@ -144,6 +163,8 @@
     head_count = state_mem.shape[1]
     head_size = state_mem.shape[3]
     inner_width = head_count * head_size
+    first_side = lax.axis_index("tp") == 0
+    live_mask, later, total = block_gates(fgate_blk, lengths)
     gathered = lax.all_gather(tokens, "tp", axis=0, tiled=True)
     widened = gathered.astype(jnp.float32)
     square_in = jnp.sum(widened * widened, axis=1)
@@ -153,9 +174,10 @@
     main_part = jnp.dot(scaled_in, w_main, preferred_element_type=jnp.float32)
     gate_part = jnp.dot(scaled_in, w_gates, preferred_element_type=jnp.float32)
     extras_in = jnp.concatenate([gate_part, square_in[:, None]], axis=1)
-    main_sum, extra_sum = scatter_sum(
-        with_extras(main_part, extras_in), main_part.shape[1], extras_in.shape[1]
-    )
+    packed, first_side, live_mask, later, total = lax.optimization_barrier(
+        (with_extras(main_part, extras_in), first_side, live_mask, later, total)
+    )
+    main_sum, extra_sum = scatter_sum(packed, main_part.shape[1], extras_in.shape[1])
     gate_sum = extra_sum[:, : 2 * head_count]
     square_mine = extra_sum[:, 2 * head_count]
     factor_in = lax.rsqrt(square_mine / D + EPS)[:, None]
@@ -187,8 +209,9 @@
         keys_blk,
         values_blk,
         igate_blk,
-        fgate_blk,
-        lengths,
+        live_mask,
+        later,
+        total,
         gain_head,
     )
     partial_value = jnp.dot(
@@ -208,8 +231,8 @@
     )
     down_part = jnp.dot(gather_rows(hidden), w_down, preferred_element_type=jnp.float32)
     row_count = tokens.shape[0]
-    down_sum = tp_scatter_sum(down_part.astype(jnp.bfloat16), row_count)
-    own_rows = lax.dynamic_slice_in_dim(restored, lax.axis_index("tp") * row_count, row_count, 0)
+    down_sum = tp_scatter_sum(down_part.astype(jnp.bfloat16), row_count, first_side)
+    own_rows = own_half(restored, row_count, first_side)
     return (own_rows + down_sum).astype(jnp.bfloat16)
 
 

time: 89.2 us -> 88.9 us (level)
  blocking collectives: 33.3 us -> 72.1 us
  waiting for transfers between devices: 28.5 us -> 2.33 us
  starting transfers between devices: 11.9 us -> 0.14 us
  local copies, waits for them, and re-layouts: 2.79 us -> 1.08 us
  other arithmetic: 4.1 us -> 5.11 us
    all_to_all x2 -> x0, waiting for transfers between devices: 26.2 us -> none  [the longest x1 14.5 us: gather_rows(): lax.all_to_all(copies, 'kv', 0, 0, tiled=True).reshape(-1, rows.shape[1])]
    all_to_all x1 -> x2, blocking collectives: 19.7 us -> 41.1 us  [scatter_sum(): received = lax.all_to_all(blocks, 'kv', 0, 0, tiled=True)]
    all_to_all x1 -> x2, blocking collectives: 11.3 us -> 28.8 us  [gather_rows(): lax.all_to_all(copies, 'kv', 0, 0, tiled=True).reshape(-1, rows.shape[1])]
    all_to_all x2 -> x0, starting transfers between devices: 11.8 us -> none  [the longest x1 8.19 us: scatter_sum(): received = lax.all_to_all(blocks, 'kv', 0, 0, tiled=True)]
    lt x1 -> x2, other arithmetic: 0.07 us -> 1.54 us  [block_gates(): live_mask = positions[None, None, :] < lengths[:, None, None]]
    another operation x4 -> x3, other arithmetic: 1.34 us -> 0.11 us  [the longest x1 1.23 us: memory_cell(): cumulative = jnp.cumsum(forget_live, axis=-1)]
    dot_general x1 -> x2, matrix products: 4.22 us -> 3.76 us  [the longest x1 2.92 us: memory_cell(): jnp.einsum('shvk,shk->shv', state_mem.astype(jnp.bfloat16), query, prefer...]
  transfers between devices with their start and end apart: 4 -> 2, of which waited for: 4 -> 2; matrix products, arithmetic and copies ran while one was open for 2% -> 0% of each run, Pallas kernels for 0% -> 0%
where the time goes in v2:
time: 88.9 us; the launch traced here: 88.4 us
  blocking collectives  72.1 us (81%)
  matrix products  7.38 us (8%)
  other arithmetic  5.11 us (6%)
  waiting for transfers between devices  2.33 us (3%)
  local copies, waits for them, and re-layouts  1.08 us (1%)
    all_to_all x2, blocking collectives, scatter_sum(): received = lax.all_to_all(blocks, 'kv', 0, 0, tiled=True)  41.1 us
    all_to_all x2, blocking collectives, gather_rows(): lax.all_to_all(copies, 'kv', 0, 0, tiled=True).reshape(-1, rows.shape[1])  28.8 us
    dot_general x1, matrix products, memory_cell(): jnp.einsum('shvk,shk->shv', state_mem.astype(jnp.bfloat16), query, prefer...  2.92 us
    all_gather x1, blocking collectives, body(): gathered = lax.all_gather(tokens, 'tp', axis=0, tiled=True)  2.18 us
  transfers between devices with their start and end apart: 2, of which 2 were waited for; matrix products, arithmetic and copies ran while one was open for 0% of the time, Pallas kernels for 0%

profile of v2, /device:TPU:0, one launch (start us, length us, event | category | flops | bytes accessed | tf_op | source)
XLA Modules:
  0.0 88.4 jit_solution(18293392690869671072)
XLA Ops:
  0.0 0.0 copy-start
  0.0 0.8 iota_compare_fusion.3
  0.8 0.7 iota_compare_fusion.4
  1.5 0.8 select_reduce_fusion.1
  2.3 0.8 fusion.15
  3.2 2.2 %all_gather.3 = bf16[64,128]{1,0:T(8,128)(2,1)S(1)} all-gather(bf16[32,128]{1,0:T(8,128)(2,1)} %param.21), channel_id=1, replica_groups=mesh['kv'=16,'tp'=2] {'tp'}, dimensions={0}, use_global_device_ids=true | all-gather | bytes 24576 | tf_op jit(solution)/shard_map/all_gather | solution.py:168
  5.4 0.1 fusion.19
  5.5 0.8 fusion.26
  6.4 0.1 copy.40
  6.5 1.4 %convolution_convert_fusion.1 = bf16[64,3072]{1,0:T(8,128)(2,1)S(1)} fusion(bf16[128,1024]{1,0:T(8,128)(2,1)} %param.25, bf16[128,1024]{1,0:T(8,128)(2,1)} %param.24, bf16[128,1024]{1,0:T(8,128)(2,1)} %param.23, bf16[64,128]{1,0:T(8,128)(2,1)S(1)} %all_gather.3, f32[128]{0:T(128)} %param.22), kind=kOutput, calls=%fused_computation.1 | convolution fusion | flops 52912128 | bytes 1196544 | tf_op jit(solution)/shard_map/dot_general | solution.py:174
  7.9 0.0 copy-start.2
  7.9 0.1 reshape.146
  8.0 21.4 %all_to_all.20 = bf16[16,4,3200]{2,1,0:T(4,128)(2,1)S(1)} all-to-all(bf16[16,4,3200]{2,1,0:T(4,128)(2,1)S(1)} %reshape.146), channel_id=1, replica_groups=mesh['kv'=16,'tp'=2] {'kv'}, dimensions={0} | all-to-all | bytes 819200 | tf_op jit(solution)/shard_map/all_to_all | solution.py:88
  29.4 0.2 convert_reduce_fusion.1
  29.6 0.1 reshape.147
  29.7 0.2 rsqrt_reduce_fusion.1
  29.8 0.1 fusion.17
  29.9 0.1 slice_multiply_fusion.2
  30.1 0.0 copy-done.2
  30.1 0.4 fusion.51
  30.4 0.0 copy-start.7
  30.4 0.0 copy-start.5
  30.5 0.0 copy-start.6
  30.5 0.0 copy-start.8
  30.5 0.0 copy-start.3
  30.5 0.0 copy-start.9
  30.5 2.9 %fusion = f32[4,4,1,256]{3,2,1,0:T(1,128)S(1)} fusion(bf16[4,4,256,1]{2,3,1,0:T(2,128)(2,1)S(1)} %reshape.163, f32[4,4,256,256]{3,2,1,0:T(8,128)} %param.30), kind=kOutput, calls=%fused_computation.2 | convolution fusion | flops 3145728 | bytes 4218880 | tf_op jit(solution)/shard_map/shvk,shk->shv/dot_general | solution.py:48
  33.5 0.0 copy-done.7
  33.5 0.1 fusion.38
  33.6 0.0 copy-done.5
  33.6 0.2 select_reduce_fusion
  33.7 0.0 copy-done.6
  33.7 0.0 copy-done.8
  33.7 0.1 subtract_exponential_fusion
  33.8 0.1 fusion.36
  33.9 0.1 multiply_reduce_fusion.2
  34.0 0.0 copy-done.3
  34.0 0.2 fusion.32
  34.3 0.2 multiply_reduce_fusion.1
  34.5 0.0 copy-done.9
  34.5 0.1 fusion.31
  34.6 11.3 %all_to_all.21 = bf16[16,4,1024]{2,1,0:T(4,128)(2,1)S(1)} all-to-all(bf16[16,4,1024]{2,1,0:T(4,128)(2,1)S(1)} %broadcast_in_dim.65), channel_id=1, replica_groups=mesh['kv'=16,'tp'=2] {'kv'}, dimensions={0} | all-to-all | bytes 262144 | tf_op jit(solution)/shard_map/all_to_all | solution.py:98
  45.9 0.0 copy-done.4
  45.9 0.2 convolution_convert_fusion.3
  46.1 0.1 collective-permute-start
  46.2 1.2 %collective-permute-done = bf16[64,128]{1,0:T(8,128)(2,1)S(1)} collective-permute-done((bf16[64,128]{1,0:T(8,128)(2,1)S(1)}, bf16[64,128]{1,0:T(8,128)(2,1)S(1)}, u32[]{:S(2)}, u32[]{:S(2)}) %collective-permute-start) | collective-permute-done | bytes 16416 | tf_op jit(solution)/shard_map/ppermute | solution.py:104
  47.3 0.1 multiply_reduce_fusion
  47.5 0.1 copy.34
  47.6 0.0 copy-done
  47.6 0.0 copy-done.10
  47.6 0.3 convolution_convert_fusion
  48.0 0.1 reshape.150
  48.1 19.7 %all_to_all.22 = bf16[16,4,4224]{2,1,0:T(4,128)(2,1)S(1)} all-to-all(bf16[16,4,4224]{2,1,0:T(4,128)(2,1)S(1)} %reshape.150), channel_id=1, replica_groups=mesh['kv'=16,'tp'=2] {'kv'}, dimensions={0} | all-to-all | bytes 1081344 | tf_op jit(solution)/shard_map/all_to_all | solution.py:88
  67.8 0.2 convert_reduce_fusion
  68.0 0.2 rsqrt_reduce_fusion
  68.2 0.1 fusion.13
  68.3 0.2 broadcast_in_dim.66
  68.5 17.6 %all_to_all.23 = bf16[16,4,4096]{2,1,0:T(4,128)(2,1)S(1)} all-to-all(bf16[16,4,4096]{2,1,0:T(4,128)(2,1)S(1)} %broadcast_in_dim.66), channel_id=1, replica_groups=mesh['kv'=16,'tp'=2] {'kv'}, dimensions={0} | all-to-all | bytes 1048576 | tf_op jit(solution)/shard_map/all_to_all | solution.py:98
  86.1 0.1 reshape.152
  86.2 0.0 copy-done.1
  86.2 0.3 convolution_convert_fusion.2
  86.6 0.1 collective-permute-start.1
  86.7 1.2 %collective-permute-done.1 = bf16[32,128]{1,0:T(8,128)(2,1)S(1)} collective-permute-done((bf16[32,128]{1,0:T(8,128)(2,1)S(1)}, bf16[32,128]{1,0:T(8,128)(2,1)S(1)}, u32[]{:S(2)}, u32[]{:S(2)}) %collective-permute-start.1) | collective-permute-done | bytes 8224 | tf_op jit(solution)/shard_map/ppermute | solution.py:125
  87.8 0.6 fusion.23
  (23 shorter events, 0.3 us)
Async XLA Ops:
  0.0 47.6 %copy-start = (bf16[128,4096]{1,0:T(8,128)(2,1)S(1)}, bf16[128,4096]{1,0:T(8,128)(2,1)}, u32[]{:S(2)}) copy-start(bf16[128,4096]{1,0:T(8,128)(2,1)} %param.40) | copy-start | bytes 3145732
  7.9 22.2 %copy-start.2 = (bf16[4,4,128,256]{3,2,1,0:T(8,128)(2,1)S(1)}, bf16[4,4,128,256]{3,2,1,0:T(8,128)(2,1)}, u32[]{:S(2)}) copy-start(bf16[4,4,128,256]{3,2,1,0:T(8,128)(2,1)} %param.32) | copy-start | bytes 3145732
  30.4 3.0 %copy-start.7 = (f32[4]{0:T(128)S(1)}, f32[4]{0:T(128)}, u32[]{:S(2)}) copy-start(f32[4]{0:T(128)} %param.29) | copy-start | bytes 52
  30.4 3.1 %copy-start.5 = (f32[4,4,128]{2,1,0:T(4,128)S(1)}, f32[4,4,128]{2,1,0:T(4,128)}, u32[]{:S(2)}) copy-start(f32[4,4,128]{2,1,0:T(4,128)} %param.34) | copy-start | bytes 24580
  30.5 3.3 %copy-start.6 = (f32[4,4]{1,0:T(4,128)S(1)}, f32[4,4]{1,0:T(4,128)}, u32[]{:S(2)}) copy-start(f32[4,4]{1,0:T(4,128)} %param.31) | copy-start | bytes 196
  30.5 3.3 %copy-start.8 = (f32[4]{0:T(128)S(1)}, f32[4]{0:T(128)}, u32[]{:S(2)}) copy-start(f32[4]{0:T(128)} %param.28) | copy-start | bytes 52
  30.5 3.6 %copy-start.3 = (bf16[4,4,128,256]{3,2,1,0:T(8,128)(2,1)S(1)}, bf16[4,4,128,256]{3,2,1,0:T(8,128)(2,1)}, u32[]{:S(2)}) copy-start(bf16[4,4,128,256]{3,2,1,0:T(8,128)(2,1)} %param.33) | copy-start | bytes 3145732
  30.5 4.0 %copy-start.9 = (f32[256]{0:T(256)S(1)}, f32[256]{0:T(256)}, u32[]{:S(2)}) copy-start(f32[256]{0:T(256)} %param.37) | copy-start | bytes 3076
  33.4 12.5 %copy-start.4 = (bf16[1024,128]{1,0:T(8,128)(2,1)S(1)}, bf16[1024,128]{1,0:T(8,128)(2,1)}, u32[]{:S(2)}) copy-start(bf16[1024,128]{1,0:T(8,128)(2,1)} %param.38) | copy-start | bytes 786436
  33.4 14.2 %copy-start.10 = (f32[128]{0:T(128)S(1)}, f32[128]{0:T(128)}, u32[]{:S(2)}) copy-start(f32[128]{0:T(128)} %param.39) | copy-start | bytes 1540
  46.1 1.2 %collective-permute-start = (bf16[64,128]{1,0:T(8,128)(2,1)S(1)}, bf16[64,128]{1,0:T(8,128)(2,1)S(1)}, u32[]{:S(2)}, u32[]{:S(2)}) collective-permute-start(bf16[64,128]{1,0:T(8,128)(2,1)S(1)} %convolution_convert_fusion.3), channel_id=1, source_target_pairs={{0,1},{1,0},{2,3},{3,2},{4,5},{5,4},{6,7},{7,6},{8,9},{9,8},{10,11... | collective-permute-start | bytes 49160 | tf_op jit(solution)/shard_map/ppermute | solution.py:104
  67.8 18.4 %copy-start.1 = (bf16[4096,128]{1,0:T(8,128)(2,1)S(1)}, bf16[4096,128]{1,0:T(8,128)(2,1)}, u32[]{:S(2)}) copy-start(bf16[4096,128]{1,0:T(8,128)(2,1)} %param.41) | copy-start | bytes 3145732
  86.6 1.2 %collective-permute-start.1 = (bf16[32,128]{1,0:T(8,128)(2,1)S(1)}, bf16[32,128]{1,0:T(8,128)(2,1)S(1)}, u32[]{:S(2)}, u32[]{:S(2)}) collective-permute-start(bf16[32,128]{1,0:T(8,128)(2,1)S(1)} %broadcast_select_fusion), channel_id=1, source_target_pairs={{0,1},{1,0},{2,3},{3,2},{4,5},{5,4},{6,7},{7,6},{8,9},{9,8},{10,11... | collective-permute-start | bytes 24584 | tf_op jit(solution)/shard_map/ppermute | solution.py:125

commit v3 on v2

--- a/solution.py
+++ b/solution.py
@@ -164,20 +164,26 @@
     head_size = state_mem.shape[3]
     inner_width = head_count * head_size
     first_side = lax.axis_index("tp") == 0
-    live_mask, later, total = block_gates(fgate_blk, lengths)
     gathered = lax.all_gather(tokens, "tp", axis=0, tiled=True)
     widened = gathered.astype(jnp.float32)
     square_in = jnp.sum(widened * widened, axis=1)
     scaled_in = (widened * gain_mix).astype(jnp.bfloat16)
     w_main = jnp.concatenate([w_query, w_key, w_value], axis=1)
+    main_part = jnp.dot(scaled_in, w_main, preferred_element_type=jnp.float32)
+    main_part, w_igate, w_fgate = lax.optimization_barrier(
+        (main_part.astype(jnp.bfloat16), w_igate, w_fgate)
+    )
     w_gates = jnp.concatenate([w_igate, w_fgate], axis=1)
-    main_part = jnp.dot(scaled_in, w_main, preferred_element_type=jnp.float32)
     gate_part = jnp.dot(scaled_in, w_gates, preferred_element_type=jnp.float32)
     extras_in = jnp.concatenate([gate_part, square_in[:, None]], axis=1)
-    packed, first_side, live_mask, later, total = lax.optimization_barrier(
-        (with_extras(main_part, extras_in), first_side, live_mask, later, total)
+    packed, first_side = lax.optimization_barrier(
+        (with_extras(main_part, extras_in), first_side)
     )
     main_sum, extra_sum = scatter_sum(packed, main_part.shape[1], extras_in.shape[1])
+    main_sum, extra_sum, fgate_blk, lengths = lax.optimization_barrier(
+        (main_sum, extra_sum, fgate_blk, lengths)
+    )
+    live_mask, later, total = block_gates(fgate_blk, lengths)
     gate_sum = extra_sum[:, : 2 * head_count]
     square_mine = extra_sum[:, 2 * head_count]
     factor_in = lax.rsqrt(square_mine / D + EPS)[:, None]

time: 88.9 us -> 85.2 us (0.958)
  other arithmetic: 5.11 us -> 2.69 us
  matrix products: 7.38 us -> 6.07 us
    lt x2 -> x1, other arithmetic: 1.54 us -> 0.07 us  [block_gates(): live_mask = positions[None, None, :] < lengths[:, None, None]]
where the time goes in v3:
time: 85.2 us; the launch traced here: 84.9 us
  blocking collectives  72.2 us (85%)
  matrix products  6.07 us (7%)
  other arithmetic  2.69 us (3%)
  waiting for transfers between devices  2.33 us (3%)
  local copies, waits for them, and re-layouts  1.1 us (1%)
    all_to_all x2, blocking collectives, scatter_sum(): received = lax.all_to_all(blocks, 'kv', 0, 0, tiled=True)  41.1 us
    all_to_all x2, blocking collectives, gather_rows(): lax.all_to_all(copies, 'kv', 0, 0, tiled=True).reshape(-1, rows.shape[1])  28.8 us
    dot_general x1, matrix products, memory_cell(): jnp.einsum('shvk,shk->shv', state_mem.astype(jnp.bfloat16), query, prefer...  2.92 us
    all_gather x1, blocking collectives, body(): gathered = lax.all_gather(tokens, 'tp', axis=0, tiled=True)  2.32 us
  transfers between devices with their start and end apart: 2, of which 2 were waited for; matrix products, arithmetic and copies ran while one was open for 0% of the time, Pallas kernels for 0%

profile of v3, /device:TPU:0, one launch (start us, length us, event | category | flops | bytes accessed | tf_op | source)
XLA Modules:
  0.0 84.9 jit_solution(7051530883193845721)
XLA Ops:
  0.0 0.0 copy-start
  0.0 2.3 %all_gather.3 = bf16[64,128]{1,0:T(8,128)(2,1)S(1)} all-gather(bf16[32,128]{1,0:T(8,128)(2,1)} %param.21), channel_id=1, replica_groups=mesh['kv'=16,'tp'=2] {'tp'}, dimensions={0}, use_global_device_ids=true | all-gather | bytes 24576 | tf_op jit(solution)/shard_map/all_gather | solution.py:167
  2.3 0.1 fusion.18
  2.4 1.4 %convolution_convert_fusion.1 = bf16[64,3072]{1,0:T(8,128)(2,1)S(1)} fusion(bf16[128,1024]{1,0:T(8,128)(2,1)} %param.25, bf16[128,1024]{1,0:T(8,128)(2,1)} %param.24, bf16[128,1024]{1,0:T(8,128)(2,1)} %param.23, bf16[64,128]{1,0:T(8,128)(2,1)S(1)} %all_gather.3, f32[128]{0:T(128)} %param.22), kind=kOutput, calls=%fused_computation.1 | convolution fusion | flops 52912128 | bytes 1196544 | tf_op jit(solution)/shard_map/dot_general | solution.py:172
  3.8 0.0 copy-done.12
  3.9 0.0 copy-done.9
  3.9 0.0 copy-done.10
  3.9 0.1 fusion.25
  4.0 0.1 copy.40
  4.2 0.0 copy-start.2
  4.2 0.1 reshape.132
  4.3 21.4 %all_to_all.20 = bf16[16,4,3200]{2,1,0:T(4,128)(2,1)S(1)} all-to-all(bf16[16,4,3200]{2,1,0:T(4,128)(2,1)S(1)} %reshape.132), channel_id=1, replica_groups=mesh['kv'=16,'tp'=2] {'kv'}, dimensions={0} | all-to-all | bytes 819200 | tf_op jit(solution)/shard_map/all_to_all | solution.py:88
  25.7 0.2 convert_reduce_fusion.1
  25.9 0.1 reshape.133
  26.0 0.2 rsqrt_reduce_fusion.1
  26.1 0.1 slice_multiply_fusion.1
  26.2 0.1 multiply_convert_fusion
  26.4 0.0 copy-done.15
  26.4 0.1 iota_compare_fusion.3
  26.5 0.0 copy-done.2
  26.5 0.4 fusion.50
  26.9 0.0 copy-start.5
  26.9 0.0 copy-start.7
  26.9 0.0 copy-start.3
  26.9 0.0 copy-start.8
  26.9 2.9 %fusion = f32[4,4,1,256]{3,2,1,0:T(1,128)S(1)} fusion(bf16[4,4,256,1]{2,3,1,0:T(2,128)(2,1)S(1)} %reshape.149, f32[4,4,256,256]{3,2,1,0:T(8,128)} %param.30), kind=kOutput, calls=%fused_computation.2 | convolution fusion | flops 3145728 | bytes 4218880 | tf_op jit(solution)/shard_map/shvk,shk->shv/dot_general | solution.py:48
  29.9 0.0 copy-done.6
  29.9 0.1 fusion.37
  30.0 0.1 multiply_reduce_fusion.2
  30.1 0.0 copy-done.13
  30.1 0.0 copy-done.14
  30.1 0.2 select_reduce_fusion.1
  30.3 0.0 copy-done.5
  30.3 0.0 copy-done.7
  30.3 0.1 subtract_exponential_fusion
  30.4 0.1 fusion.35
  30.5 0.0 copy-done.3
  30.5 0.2 fusion.31
  30.8 0.2 multiply_reduce_fusion.1
  31.0 0.0 copy-done.8
  31.0 0.1 fusion.30
  31.1 11.3 %all_to_all.21 = bf16[16,4,1024]{2,1,0:T(4,128)(2,1)S(1)} all-to-all(bf16[16,4,1024]{2,1,0:T(4,128)(2,1)S(1)} %broadcast_in_dim.59), channel_id=1, replica_groups=mesh['kv'=16,'tp'=2] {'kv'}, dimensions={0} | all-to-all | bytes 262144 | tf_op jit(solution)/shard_map/all_to_all | solution.py:98
  42.4 0.0 copy-done.4
  42.4 0.2 convolution_convert_fusion.3
  42.6 0.1 collective-permute-start
  42.7 1.2 %collective-permute-done = bf16[64,128]{1,0:T(8,128)(2,1)S(1)} collective-permute-done((bf16[64,128]{1,0:T(8,128)(2,1)S(1)}, bf16[64,128]{1,0:T(8,128)(2,1)S(1)}, u32[]{:S(2)}, u32[]{:S(2)}) %collective-permute-start) | collective-permute-done | bytes 16416 | tf_op jit(solution)/shard_map/ppermute | solution.py:104
  43.8 0.1 multiply_reduce_fusion
  44.0 0.1 copy.34
  44.1 0.0 copy-done
  44.1 0.0 copy-done.11
  44.1 0.3 convolution_convert_fusion
  44.5 0.1 reshape.136
  44.6 19.7 %all_to_all.22 = bf16[16,4,4224]{2,1,0:T(4,128)(2,1)S(1)} all-to-all(bf16[16,4,4224]{2,1,0:T(4,128)(2,1)S(1)} %reshape.136), channel_id=1, replica_groups=mesh['kv'=16,'tp'=2] {'kv'}, dimensions={0} | all-to-all | bytes 1081344 | tf_op jit(solution)/shard_map/all_to_all | solution.py:88
  64.3 0.2 convert_reduce_fusion
  64.5 0.2 rsqrt_reduce_fusion
  64.7 0.1 fusion.14
  64.8 0.2 broadcast_in_dim.60
  65.0 17.6 %all_to_all.23 = bf16[16,4,4096]{2,1,0:T(4,128)(2,1)S(1)} all-to-all(bf16[16,4,4096]{2,1,0:T(4,128)(2,1)S(1)} %broadcast_in_dim.60), channel_id=1, replica_groups=mesh['kv'=16,'tp'=2] {'kv'}, dimensions={0} | all-to-all | bytes 1048576 | tf_op jit(solution)/shard_map/all_to_all | solution.py:98
  82.6 0.1 reshape.138
  82.7 0.0 copy-done.1
  82.7 0.3 convolution_convert_fusion.2
  83.1 0.1 collective-permute-start.1
  83.2 1.2 %collective-permute-done.1 = bf16[32,128]{1,0:T(8,128)(2,1)S(1)} collective-permute-done((bf16[32,128]{1,0:T(8,128)(2,1)S(1)}, bf16[32,128]{1,0:T(8,128)(2,1)S(1)}, u32[]{:S(2)}, u32[]{:S(2)}) %collective-permute-start.1) | collective-permute-done | bytes 8224 | tf_op jit(solution)/shard_map/ppermute | solution.py:125
  84.3 0.6 fusion.22
  (31 shorter events, 0.4 us)
Async XLA Ops:
  0.0 44.1 %copy-start = (bf16[128,4096]{1,0:T(8,128)(2,1)S(1)}, bf16[128,4096]{1,0:T(8,128)(2,1)}, u32[]{:S(2)}) copy-start(bf16[128,4096]{1,0:T(8,128)(2,1)} %param.40) | copy-start | bytes 3145732
  0.0 3.8 %copy-start.12 = (f32[128]{0:T(128)S(1)}, f32[128]{0:T(128)}, u32[]{:S(2)}) copy-start(f32[128]{0:T(128)} %param.22) | copy-start | bytes 1540
  0.0 3.8 %copy-start.9 = (bf16[128,4]{0,1:T(4,128)(2,1)S(1)}, bf16[128,4]{0,1:T(4,128)(2,1)}, u32[]{:S(2)}) copy-start(bf16[128,4]{0,1:T(4,128)(2,1)} %param.27) | copy-start | bytes 3076
  0.0 3.9 %copy-start.10 = (bf16[128,4]{0,1:T(4,128)(2,1)S(1)}, bf16[128,4]{0,1:T(4,128)(2,1)}, u32[]{:S(2)}) copy-start(bf16[128,4]{0,1:T(4,128)(2,1)} %param.26) | copy-start | bytes 3076
  4.1 22.2 %copy-start.15 = (s32[4]{0:T(128)S(1)}, s32[4]{0:T(128)}, u32[]{:S(2)}) copy-start(s32[4]{0:T(128)} %param.36) | copy-start | bytes 52
  4.2 22.3 %copy-start.2 = (bf16[4,4,128,256]{3,2,1,0:T(8,128)(2,1)S(1)}, bf16[4,4,128,256]{3,2,1,0:T(8,128)(2,1)}, u32[]{:S(2)}) copy-start(bf16[4,4,128,256]{3,2,1,0:T(8,128)(2,1)} %param.32) | copy-start | bytes 3145732
  26.8 3.0 %copy-start.6 = (f32[4]{0:T(128)S(1)}, f32[4]{0:T(128)}, u32[]{:S(2)}) copy-start(f32[4]{0:T(128)} %param.29) | copy-start | bytes 52
  26.8 3.2 %copy-start.13 = (f32[4,4,128]{2,1,0:T(4,128)S(1)}, f32[4,4,128]{2,1,0:T(4,128)}, u32[]{:S(2)}) copy-start(f32[4,4,128]{2,1,0:T(4,128)} %param.35) | copy-start | bytes 24580
  26.8 3.2 %copy-start.14 = (f32[4,4,128]{2,1,0:T(4,128)S(1)}, f32[4,4,128]{2,1,0:T(4,128)}, u32[]{:S(2)}) copy-start(f32[4,4,128]{2,1,0:T(4,128)} %param.34) | copy-start | bytes 24580
  26.9 3.5 %copy-start.5 = (f32[4,4]{1,0:T(4,128)S(1)}, f32[4,4]{1,0:T(4,128)}, u32[]{:S(2)}) copy-start(f32[4,4]{1,0:T(4,128)} %param.31) | copy-start | bytes 196
  26.9 3.4 %copy-start.7 = (f32[4]{0:T(128)S(1)}, f32[4]{0:T(128)}, u32[]{:S(2)}) copy-start(f32[4]{0:T(128)} %param.28) | copy-start | bytes 52
  26.9 3.6 %copy-start.3 = (bf16[4,4,128,256]{3,2,1,0:T(8,128)(2,1)S(1)}, bf16[4,4,128,256]{3,2,1,0:T(8,128)(2,1)}, u32[]{:S(2)}) copy-start(bf16[4,4,128,256]{3,2,1,0:T(8,128)(2,1)} %param.33) | copy-start | bytes 3145732
  26.9 4.1 %copy-start.8 = (f32[256]{0:T(256)S(1)}, f32[256]{0:T(256)}, u32[]{:S(2)}) copy-start(f32[256]{0:T(256)} %param.37) | copy-start | bytes 3076
  29.8 12.6 %copy-start.4 = (bf16[1024,128]{1,0:T(8,128)(2,1)S(1)}, bf16[1024,128]{1,0:T(8,128)(2,1)}, u32[]{:S(2)}) copy-start(bf16[1024,128]{1,0:T(8,128)(2,1)} %param.38) | copy-start | bytes 786436
  29.8 14.3 %copy-start.11 = (f32[128]{0:T(128)S(1)}, f32[128]{0:T(128)}, u32[]{:S(2)}) copy-start(f32[128]{0:T(128)} %param.39) | copy-start | bytes 1540
  42.6 1.2 %collective-permute-start = (bf16[64,128]{1,0:T(8,128)(2,1)S(1)}, bf16[64,128]{1,0:T(8,128)(2,1)S(1)}, u32[]{:S(2)}, u32[]{:S(2)}) collective-permute-start(bf16[64,128]{1,0:T(8,128)(2,1)S(1)} %convolution_convert_fusion.3), channel_id=1, source_target_pairs={{0,1},{1,0},{2,3},{3,2},{4,5},{5,4},{6,7},{7,6},{8,9},{9,8},{10,11... | collective-permute-start | bytes 49160 | tf_op jit(solution)/shard_map/ppermute | solution.py:104
  64.3 18.4 %copy-start.1 = (bf16[4096,128]{1,0:T(8,128)(2,1)S(1)}, bf16[4096,128]{1,0:T(8,128)(2,1)}, u32[]{:S(2)}) copy-start(bf16[4096,128]{1,0:T(8,128)(2,1)} %param.41) | copy-start | bytes 3145732
  83.1 1.2 %collective-permute-start.1 = (bf16[32,128]{1,0:T(8,128)(2,1)S(1)}, bf16[32,128]{1,0:T(8,128)(2,1)S(1)}, u32[]{:S(2)}, u32[]{:S(2)}) collective-permute-start(bf16[32,128]{1,0:T(8,128)(2,1)S(1)} %broadcast_select_fusion), channel_id=1, source_target_pairs={{0,1},{1,0},{2,3},{3,2},{4,5},{5,4},{6,7},{7,6},{8,9},{9,8},{10,11... | collective-permute-start | bytes 24584 | tf_op jit(solution)/shard_map/ppermute | solution.py:125
